TPU v7x, 32 devices: a whole 2x2x4 slice. The times are simulated.
32 devices in a mesh: ep: 16 (over z, y, x), tp: 2 (over core).
Axes of the slice: x: 2, y: 2, z: 4, core: 2. Of those that a mesh axis runs over, the one named last changes fastest.
Arguments:
- tokens: bfloat16 [128, 2048], P('ep'), may hold values from -6 to 6
- mixer_norm_gain: float32 [2048], replicated, may hold values from 0.1 to 1.9
- gate_projection_weight: bfloat16 [2048, 2, 2048], P(None, 'tp', 'ep'), may hold values from -0.125 to 0.125
- value_projection_weight: bfloat16 [2048, 2, 2048], P(None, 'tp', 'ep'), may hold values from -0.125 to 0.125
- input_projection_weight: bfloat16 [2048, 1024], P(None, 'tp'), may hold values from -0.125 to 0.125
- output_projection_weight: bfloat16 [2048, 1024], P(None, 'tp'), may hold values from -0.125 to 0.125
- step_projection_weight: bfloat16 [2048, 64], P(None, 'tp'), may hold values from -0.125 to 0.125
- head_step_bias: float32 [64], P('tp'), may hold values from -1 to 1
- head_decay_rate: float32 [64], P('tp'), may hold values from 0.02 to 3
- extra_log_decay: float32 [128, 64], P('ep', 'tp'), may hold values from -0.7 to 0
- value_taps: float32 [4, 4096], P(None, 'tp'), may hold values from -3 to 3
- input_taps: float32 [4, 1024], P(None, 'tp'), may hold values from -3 to 3
- output_taps: float32 [4, 1024], P(None, 'tp'), may hold values from -3 to 3
- prior_values: bfloat16 [128, 3, 4096], P('ep', None, 'tp'), may hold values from -6 to 6
- prior_input_maps: bfloat16 [128, 3, 1024], P('ep', None, 'tp'), may hold values from -6 to 6
- prior_output_maps: bfloat16 [128, 3, 1024], P('ep', None, 'tp'), may hold values from -6 to 6
- head_skip_gain: float32 [64], P('tp'), may hold values from 0.5 to 1.5
- group_norm_gain: float32 [4096], P('tp'), may hold values from 0.1 to 1.9
- mixer_output_weight: bfloat16 [4096, 2048], P('tp', 'ep'), may hold values from -0.09375 to 0.09375
- recurrent_state: float32 [128, 64, 64, 128], P('ep', 'tp'), may hold values from -6 to 6
- expert_norm_gain: float32 [2048], replicated, may hold values from 0.1 to 1.9
- routes: int32 [128, 6], P('ep'), may hold values from 0 to 15, all different within a row; in each aligned block of 8 rows (0 to 7, 8 to 15, ...) at most 4 rows name the same one
- chosen_expert_weight: float32 [128, 6], P('ep'), may hold values from 0.2 to 1
- routed_gate_weight: bfloat16 [16, 2048, 512], P('ep', None, 'tp'), may hold values from -0.125 to 0.125
- routed_up_weight: bfloat16 [16, 2048, 512], P('ep', None, 'tp'), may hold values from -0.125 to 0.125
- routed_down_weight: bfloat16 [16, 512, 2048], P('ep', 'tp'), may hold values from -0.25 to 0.25
- common_gate_weight: bfloat16 [2048, 512], P(None, 'tp'), may hold values from -0.125 to 0.125
- common_up_weight: bfloat16 [2048, 512], P(None, 'tp'), may hold values from -0.125 to 0.125
- common_down_weight: bfloat16 [512, 2048], P('tp'), may hold values from -0.25 to 0.25
Outputs:
- result: bfloat16 [128, 2048], P('ep')
- state_next: float32 [128, 64, 64, 128], P('ep', 'tp')
- next_value: bfloat16 [128, 3, 4096], P('ep', None, 'tp')
- next_input: bfloat16 [128, 3, 1024], P('ep', None, 'tp')
- next_output: bfloat16 [128, 3, 1024], P('ep', None, 'tp')
Inputs may be any that keep to these rules, and one draw needn't show every extreme that they name: `routes`: the 6 experts of a row differ; among the rows of one device (aligned blocks of 8 rows) no expert is named more than 4 times.
All inputs are finite; a program needn't handle non-finite values.
Results may differ from a plain program's by a relative error of at most 0.015.
Values may be sent and summed in bfloat16 or wider, within the bound.
No kernel may reach another device: no remote copies, remote signals or barrier semaphores. Data moves between devices by JAX's collectives and lax.ppermute only.
A program may use at most 128 MiB of HBM per device.

v0:
```python
import jax
import jax.numpy as jnp
from jax import lax
from jax.sharding import PartitionSpec as P

D_INNER = 4096
GROUPS = 8
EPSILON = 1e-06


def rms_scale(values, gain_vec):
    values = values.astype(jnp.float32)
    return (
        values * lax.rsqrt(jnp.mean(values * values, axis=-1, keepdims=True) + EPSILON) * gain_vec
    )


def short_conv(past_rows, fresh_row, weight):
    window = jnp.concatenate([past_rows, fresh_row[:, None, :]], axis=1)
    summed = window[:, 0].astype(jnp.float32) * weight[0]
    for offset in range(1, window.shape[1]):
        summed = summed + window[:, offset].astype(jnp.float32) * weight[offset]
    return (jax.nn.silu(summed), window[:, 1:])


def state_step(
    state_prev, value_conv, input_conv, output_conv, timestep_size, step_decay, head_skip_gain
):
    batch_rows, head_count, head_size, state_size = state_prev.shape
    per_group = head_count // (input_conv.shape[1] // state_size)
    value_heads = value_conv.reshape(batch_rows, head_count, head_size)
    input_heads = jnp.repeat(input_conv.reshape(batch_rows, -1, state_size), per_group, axis=1)
    output_heads = jnp.repeat(output_conv.reshape(batch_rows, -1, state_size), per_group, axis=1)
    state_next = (
        step_decay[:, :, None, None] * state_prev
        + (timestep_size[:, :, None] * value_heads)[:, :, :, None] * input_heads[:, :, None, :]
    )
    mixed_heads = (
        jnp.sum(state_next * output_heads[:, :, None, :], axis=-1)
        + head_skip_gain[None, :, None] * value_heads
    )
    return (state_next, mixed_heads.reshape(batch_rows, -1))


def gated_norm(mixed_flat, gate_rows, group_norm_gain, group_width):
    gated_rows = mixed_flat * jax.nn.silu(gate_rows.astype(jnp.float32))
    grouped = gated_rows.reshape(gated_rows.shape[0], -1, group_width)
    grouped = grouped * lax.rsqrt(jnp.mean(grouped * grouped, axis=-1, keepdims=True) + EPSILON)
    return (grouped.reshape(gated_rows.shape[0], -1) * group_norm_gain).astype(jnp.bfloat16)


def expert_partial(arrived, gate_mat, up_mat, down_mat):
    gate_part = jnp.einsum("slcd,ldf->slcf", arrived, gate_mat, preferred_element_type=jnp.float32)
    up_part = jnp.einsum("slcd,ldf->slcf", arrived, up_mat, preferred_element_type=jnp.float32)
    hidden = (jax.nn.silu(gate_part) * up_part).astype(jnp.bfloat16)
    return jnp.einsum("slcf,lfd->slcd", hidden, down_mat, preferred_element_type=jnp.float32)


def shards(
    tokens,
    mixer_norm_gain,
    gate_projection_weight,
    value_projection_weight,
    input_projection_weight,
    output_projection_weight,
    step_projection_weight,
    head_step_bias,
    head_decay_rate,
    extra_log_decay,
    value_taps,
    input_taps,
    output_taps,
    prior_values,
    prior_input_maps,
    prior_output_maps,
    head_skip_gain,
    group_norm_gain,
    mixer_output_weight,
    recurrent_state,
    expert_norm_gain,
    routes,
    chosen_expert_weight,
    routed_gate_weight,
    routed_up_weight,
    routed_down_weight,
    common_gate_weight,
    common_up_weight,
    common_down_weight,
):
    seq_rows, model_width = tokens.shape
    ep_count = lax.axis_size("ep")
    tp_count = lax.axis_size("tp")
    tp_place = lax.axis_index("tp")
    normed = rms_scale(tokens, mixer_norm_gain).astype(jnp.bfloat16)
    both_pieces = jnp.concatenate(
        [
            gate_projection_weight.reshape(model_width, -1),
            value_projection_weight.reshape(model_width, -1),
        ],
        axis=1,
    )
    piece_width = both_pieces.shape[1] // 2
    projected = jnp.dot(
        lax.all_gather(normed, "ep", axis=0, tiled=True),
        both_pieces,
        preferred_element_type=jnp.float32,
    ).astype(jnp.bfloat16)
    returned = lax.all_to_all(projected, "ep", split_axis=0, concat_axis=1, tiled=True).reshape(
        seq_rows, ep_count, 2, piece_width
    )
    gate_rows = returned[:, :, 0].reshape(seq_rows, -1)
    value_rows = returned[:, :, 1].reshape(seq_rows, -1)
    input_rows = jnp.dot(
        normed, input_projection_weight, preferred_element_type=jnp.float32
    ).astype(jnp.bfloat16)
    output_rows = jnp.dot(
        normed, output_projection_weight, preferred_element_type=jnp.float32
    ).astype(jnp.bfloat16)
    step_raw = jnp.dot(normed, step_projection_weight, preferred_element_type=jnp.float32)
    value_conv, next_value = short_conv(prior_values, value_rows, value_taps)
    input_conv, next_input = short_conv(prior_input_maps, input_rows, input_taps)
    output_conv, next_output = short_conv(prior_output_maps, output_rows, output_taps)
    timestep_size = jax.nn.softplus(step_raw + head_step_bias)
    step_decay = jnp.exp(-timestep_size * head_decay_rate + extra_log_decay)
    state_next, mixed_flat = state_step(
        recurrent_state,
        value_conv,
        input_conv,
        output_conv,
        timestep_size,
        step_decay,
        head_skip_gain,
    )
    mixer_rows = gated_norm(mixed_flat, gate_rows, group_norm_gain, D_INNER // GROUPS)
    partial_mix = jnp.dot(
        lax.all_gather(mixer_rows, "ep", axis=0, tiled=True),
        mixer_output_weight,
        preferred_element_type=jnp.float32,
    )
    mix_share = lax.psum_scatter(
        partial_mix.reshape(ep_count, seq_rows, -1).astype(jnp.bfloat16),
        "tp",
        scatter_dimension=1,
        tiled=True,
    )
    moved_mix = lax.all_to_all(mix_share, "ep", split_axis=0, concat_axis=2, tiled=True)
    mixed_out = lax.all_gather(moved_mix, "tp", axis=1, tiled=True).reshape(seq_rows, model_width)
    stream = (tokens.astype(jnp.float32) + mixed_out.astype(jnp.float32)).astype(jnp.bfloat16)
    ffn_rows = rms_scale(stream, expert_norm_gain).astype(jnp.bfloat16)
    shared_hidden = (
        jax.nn.silu(jnp.dot(ffn_rows, common_gate_weight, preferred_element_type=jnp.float32))
        * jnp.dot(ffn_rows, common_up_weight, preferred_element_type=jnp.float32)
    ).astype(jnp.bfloat16)
    shared_out = lax.psum(
        jnp.dot(shared_hidden, common_down_weight, preferred_element_type=jnp.float32).astype(
            jnp.bfloat16
        ),
        "tp",
    ).astype(jnp.float32)
    exp_local = routed_gate_weight.shape[0]
    expert_total = exp_local * ep_count
    topk_count = routes.shape[1]
    capacity = (seq_rows * topk_count + expert_total - 1) // expert_total + 1
    slot_count = expert_total * capacity
    expert_ids = jnp.arange(expert_total, dtype=jnp.int32)
    flat_routes = routes.reshape(-1)
    onehot = (flat_routes[:, None] == expert_ids[None, :]).astype(jnp.int32)
    slot_ids = jnp.sum((jnp.cumsum(onehot, axis=0) - onehot) * onehot, axis=1)
    positions = flat_routes * capacity + slot_ids
    matches = (jnp.arange(slot_count, dtype=jnp.int32)[:, None] == positions[None, :]).reshape(
        slot_count, seq_rows, topk_count
    )
    dispatch_mat = jnp.sum(matches.astype(jnp.float32), axis=2).astype(jnp.bfloat16)
    combine_mat = jnp.sum(jnp.where(matches, chosen_expert_weight[None], 0.0), axis=2)
    outgoing = jnp.dot(dispatch_mat, ffn_rows, preferred_element_type=jnp.float32).astype(
        jnp.bfloat16
    )
    outgoing = outgoing.reshape(ep_count, exp_local, capacity, model_width)
    half_width = model_width // tp_count
    own_cols = lax.dynamic_slice_in_dim(outgoing, tp_place * half_width, half_width, 3)
    full_rows = lax.all_gather(
        lax.all_to_all(own_cols, "ep", split_axis=0, concat_axis=0, tiled=True),
        "tp",
        axis=3,
        tiled=True,
    )
    partial_out = expert_partial(
        full_rows, routed_gate_weight, routed_up_weight, routed_down_weight
    )
    share_out = lax.psum_scatter(
        partial_out.astype(jnp.bfloat16), "tp", scatter_dimension=3, tiled=True
    )
    back_half = lax.all_to_all(share_out, "ep", split_axis=0, concat_axis=0, tiled=True)
    routed_half = lax.dot_general(
        combine_mat,
        back_half.reshape(slot_count, half_width).astype(jnp.float32),
        (((0,), (0,)), ((), ())),
        precision=lax.Precision.HIGHEST,
    )
    routed = lax.all_gather(routed_half.astype(jnp.bfloat16), "tp", axis=1, tiled=True).astype(
        routed_half.dtype
    )
    result = (stream.astype(jnp.float32) + shared_out + routed).astype(jnp.bfloat16)
    return (result, state_next, next_value, next_input, next_output)


def solution(mesh):
    return jax.shard_map(
        shards,
        mesh=mesh,
        in_specs=(
            P("ep", None),
            P(),
            P(None, "tp", "ep"),
            P(None, "tp", "ep"),
            P(None, "tp"),
            P(None, "tp"),
            P(None, "tp"),
            P("tp"),
            P("tp"),
            P("ep", "tp"),
            P(None, "tp"),
            P(None, "tp"),
            P(None, "tp"),
            P("ep", None, "tp"),
            P("ep", None, "tp"),
            P("ep", None, "tp"),
            P("tp"),
            P("tp"),
            P("tp", "ep"),
            P("ep", "tp", None, None),
            P(),
            P("ep", None),
            P("ep", None),
            P("ep", None, "tp"),
            P("ep", None, "tp"),
            P("ep", "tp", None),
            P(None, "tp"),
            P(None, "tp"),
            P("tp", None),
        ),
        out_specs=(
            P("ep", None),
            P("ep", "tp", None, None),
            P("ep", None, "tp"),
            P("ep", None, "tp"),
            P("ep", None, "tp"),
        ),
        check_vma=False,
    )
```

profile of v0, /device:TPU:0, one launch (start us, length us, event | category | flops | bytes accessed | tf_op | source)
XLA Modules:
  0.0 206.3 jit_solution(9300064261054911112)
XLA Ops:
  7.3 1.0 fusion.18
  8.3 0.8 fusion.20
  9.1 45.3 %all_gather.15 = bf16[128,2048]{1,0:T(8,128)(2,1)S(1)} all-gather(bf16[8,2048]{1,0:T(8,128)(2,1)S(1)} %fusion.20), channel_id=1, replica_groups=mesh['ep'=16,'tp'=2] {'ep'}, dimensions={0}, use_global_device_ids=true | all-gather | bytes 557056 | tf_op jit(solution)/shard_map/all_gather | solution.py:104
  54.5 2.2 %fusion.1 = bf16[16,8,256]{2,1,0:T(8,128)(2,1)} fusion(bf16[128,2048]{1,0:T(8,128)(2,1)S(1)} %all_gather.15, bf16[2048,128]{1,0:T(8,128)(2,1)} %bitcast.213, bf16[2048,128]{1,0:T(8,128)(2,1)} %bitcast.214), kind=kOutput, calls=%fused_computation.7 | convolution fusion | flops 136347648 | bytes 1638400 | tf_op jit(solution)/shard_map/dot_general | solution.py:103
  56.6 3.5 %all-to-all-start = ((bf16[16,8,256]{2,1,0:T(8,128)(2,1)}), bf16[16,8,256]{2,1,0:T(8,128)(2,1)S(1)}, u32[]{:S(2)}, u32[]{:S(2)}) async-start(bf16[16,8,256]{2,1,0:T(8,128)(2,1)} %fusion.1), calls=%async_computation | async-start | bytes 131072 | tf_op jit(solution)/shard_map/all_to_all | solution.py:108
  60.2 1.6 slice_reduce_fusion.3
  62.0 0.8 slice_convert_fusion.2
  62.8 0.1 reshape.313
  62.9 0.1 reshape.314
  63.0 0.1 reshape.315
  63.1 0.4 convolution_convert_fusion.7
  63.5 0.9 fusion.68
  64.3 0.8 multiply_bitcast_fusion.1
  65.1 2.0 convolution_convert_fusion.6
  67.2 0.7 mul.467
  68.1 0.2 select_reduce_fusion.1
  68.3 0.7 reduce_sum.82
  69.1 0.2 add_exponential_fusion
  69.3 0.9 slice_reduce_fusion.4
  70.1 1.0 fusion.65
  71.1 0.8 copy_convert_fusion
  71.9 0.1 reshape.316
  72.0 0.7 reshape.328
  72.7 0.7 broadcast_multiply_fusion
  73.4 9.4 %multiply_reduce_fusion = (f32[8,32,64]{2,1,0:T(8,128)S(1)}, f32[8,32,64,128]{3,2,1,0:T(8,128)}) fusion(f32[8,32,128]{2,1,0:T(8,128)S(1)} %get-tuple-element.41, f32[8,32,128]{2,1,0:T(8,128)S(1)} %get-tuple-element.42, f32[8,32,64]{2,1,0:T(8,128)S(1)} %get-tuple-element.15, f32[8,32,64,128]{3,2,1,0:T(8,128)} %param.48, f32[8,32]{1,0:T(8,128)S(1)} %get-tuple-element.35), kind=kLoop, calls=%fused_computation | loop fusion | flops 10469376 | bytes 17171456 | tf_op jit(solution)/shard_map/reduce_sum | solution.py:39
  82.8 0.1 reduce_sum.76
  82.9 1.2 multiply_reduce_fusion.1
  84.1 0.1 reduce_sum.78
  84.2 0.1 reduce_sum.79
  84.3 0.1 copy.108
  84.4 1.0 fusion.41
  85.4 44.1 %all_gather.16 = bf16[128,2048]{1,0:T(8,128)(2,1)S(1)} all-gather(bf16[8,2048]{1,0:T(8,128)(2,1)S(1)} %fusion.41), channel_id=1, replica_groups=mesh['ep'=16,'tp'=2] {'ep'}, dimensions={0}, use_global_device_ids=true | all-gather | bytes 557056 | tf_op jit(solution)/shard_map/all_gather | solution.py:136
  129.5 1.3 fusion.5
  130.8 0.6 copy.98
  131.5 0.7 multiply_add_fusion.1
  132.2 0.1 copy.102
  132.3 0.8 copy.103
  133.0 2.0 reduce-scatter.3.cloned.1.call-done
  135.1 1.3 copy.99
  136.4 6.7 %all-to-all-start.1 = ((bf16[16,4,128]{2,1,0:T(4,128)(2,1)}), bf16[16,4,128]{2,1,0:T(4,128)(2,1)S(1)}, u32[]{:S(2)}, u32[]{:S(2)}) async-start(bf16[16,4,128]{2,1,0:T(4,128)(2,1)} %copy.99), calls=%async_computation.2 | async-start | bytes 32768 | tf_op jit(solution)/shard_map/all_to_all | solution.py:146
  143.2 0.7 convert_reduce_fusion
  143.8 6.6 %all-to-all-done.1 = bf16[16,4,128]{2,1,0:T(4,128)(2,1)S(1)} async-done(((bf16[16,4,128]{2,1,0:T(4,128)(2,1)}), bf16[16,4,128]{2,1,0:T(4,128)(2,1)S(1)}, u32[]{:S(2)}, u32[]{:S(2)}) %all-to-all-start.1) | async-done | bytes 16416 | tf_op jit(solution)/shard_map/all_to_all | solution.py:146
  150.5 1.9 all_gather.17
  152.3 0.9 fusion.22
  153.2 0.6 copy-done.9
  153.8 1.0 convolution_convert_fusion.1
  154.8 0.8 reshape.306
  155.6 0.9 constant_dynamic-slice_fusion
  156.5 10.6 %all_to_all.44 = bf16[16,1,4,1024]{3,2,1,0:T(4,128)(2,1)S(1)} all-to-all(bf16[16,1,4,1024]{3,2,1,0:T(4,128)(2,1)S(1)} %constant_dynamic-slice_fusion), channel_id=1, replica_groups=mesh['ep'=16,'tp'=2] {'ep'}, dimensions={0} | all-to-all | bytes 262144 | tf_op jit(solution)/shard_map/all_to_all | solution.py:182
  167.2 2.0 all_gather.18
  169.2 2.2 %convolution_bitcast_fusion.1 = f32[16,1,4,256]{3,0,2,1:T(8,128)} fusion(bf16[1,2048,256]{2,1,0:T(8,128)(2,1)} %param.52, bf16[16,1,4,2048]{3,0,2,1:T(8,128)(2,1)S(1)} %all_gather.18), kind=kOutput, calls=%fused_computation.9 | convolution fusion | flops 67108864 | bytes 1376256 | tf_op jit(solution)/shard_map/slcd,ldf->slcf/dot_general | solution.py:53
  171.4 3.1 %fusion = bf16[16,1,4,2048]{3,0,2,1:T(8,128)(2,1)} fusion(bf16[1,256,2048]{2,1,0:T(8,128)(2,1)} %param.54, bf16[1,2048,256]{2,1,0:T(8,128)(2,1)} %param.53, bf16[16,1,4,2048]{3,0,2,1:T(8,128)(2,1)S(1)} %all_gather.18, f32[16,1,4,256]{3,0,2,1:T(8,128)} %convolution_bitcast_fusion.1), kind=kOutput, calls=%fused_computation.4 | convolution fusion | flops 134447104 | bytes 2686976 | tf_op jit(solution)/shard_map/slcf,lfd->slcd/dot_general | solution.py:56
  174.5 1.4 pad_maximum_fusion.1
  175.9 1.4 pad_maximum_fusion
  177.3 1.5 fusion.63
  178.8 1.0 reduce-scatter.5.cloned.1.call-done
  179.9 1.6 copy.106
  181.5 6.7 %all-to-all-start.3 = ((bf16[16,1,4,1024]{3,2,1,0:T(4,128)(2,1)}), bf16[16,1,4,1024]{3,2,1,0:T(4,128)(2,1)S(1)}, u32[]{:S(2)}, u32[]{:S(2)}) async-start(bf16[16,1,4,1024]{3,2,1,0:T(4,128)(2,1)} %copy.106), calls=%async_computation.5 | async-start | bytes 262144 | tf_op jit(solution)/shard_map/all_to_all | solution.py:193
  188.3 2.0 convolution_convert_fusion.2
  190.2 3.4 %psum.7 = bf16[8,2048]{1,0:T(8,128)(2,1)S(1)} all-reduce(bf16[8,2048]{1,0:T(8,128)(2,1)S(1)} %convolution_convert_fusion.2), channel_id=1, replica_groups=mesh['ep'=16,'tp'=2] {'tp'}, use_global_device_ids=true, to_apply=%region_6.7 | all-reduce | flops 16384 | bytes 65536 | tf_op jit(solution)/shard_map/psum | solution.py:154
  193.7 2.5 %all-to-all-done.3 = bf16[16,1,4,1024]{3,2,1,0:T(4,128)(2,1)S(1)} async-done(((bf16[16,1,4,1024]{3,2,1,0:T(4,128)(2,1)}), bf16[16,1,4,1024]{3,2,1,0:T(4,128)(2,1)S(1)}, u32[]{:S(2)}, u32[]{:S(2)}) %all-to-all-start.3) | async-done | bytes 131104 | tf_op jit(solution)/shard_map/all_to_all | solution.py:193
  196.2 0.8 convolution_convert_fusion.5
  197.1 1.8 all_gather.19
  198.9 0.6 fusion.26
  (53 shorter events, 1.1 us)
Async XLA Ops:
  7.2 55.9 %copy-start = (bf16[2048,512]{1,0:T(8,128)(2,1)S(1)}, bf16[2048,512]{1,0:T(8,128)(2,1)}, u32[]{:S(2)}) copy-start(bf16[2048,512]{1,0:T(8,128)(2,1)} %param.33) | copy-start | bytes 6291460
  7.2 59.9 %copy-start.8 = (f32[4,512]{1,0:T(4,128)S(1)}, f32[4,512]{1,0:T(4,128)}, u32[]{:S(2)}) copy-start(f32[4,512]{1,0:T(4,128)} %param.41) | copy-start | bytes 24580
  7.2 59.9 %copy-start.4 = (bf16[8,3,512]{2,0,1:T(8,128)(2,1)S(1)}, bf16[8,3,512]{2,0,1:T(8,128)(2,1)}, u32[]{:S(2)}) copy-start(bf16[8,3,512]{2,0,1:T(8,128)(2,1)} %param.44) | copy-start | bytes 73732
  7.2 60.0 %copy-start.11 = (f32[32]{0:T(128)S(1)}, f32[32]{0:T(128)}, u32[]{:S(2)}) copy-start(f32[32]{0:T(128)} %param.45) | copy-start | bytes 388
  7.2 60.7 %copy-start.7 = (s32[8,6]{1,0:T(8,128)S(1)}, s32[8,6]{1,0:T(8,128)}, u32[]{:S(2)}) copy-start(s32[8,6]{1,0:T(8,128)} %param.50) | copy-start | bytes 580
  7.2 61.8 %copy-start.3 = (bf16[2048,32]{0,1:T(8,128)(2,1)S(1)}, bf16[2048,32]{0,1:T(8,128)(2,1)}, u32[]{:S(2)}) copy-start(bf16[2048,32]{0,1:T(8,128)(2,1)} %param.35) | copy-start | bytes 393220
  7.2 61.8 %copy-start.13 = (f32[32]{0:T(128)S(1)}, f32[32]{0:T(128)}, u32[]{:S(2)}) copy-start(f32[32]{0:T(128)} %param.36) | copy-start | bytes 388
  7.2 61.8 %copy-start.12 = (f32[32]{0:T(128)S(1)}, f32[32]{0:T(128)}, u32[]{:S(2)}) copy-start(f32[32]{0:T(128)} %param.37) | copy-start | bytes 388
  7.3 61.8 %copy-start.10 = (f32[8,32]{1,0:T(8,128)S(1)}, f32[8,32]{1,0:T(8,128)}, u32[]{:S(2)}) copy-start(f32[8,32]{1,0:T(8,128)} %param.38) | copy-start | bytes 3076
  56.6 12.6 %all-to-all-start = ((bf16[16,8,256]{2,1,0:T(8,128)(2,1)}), bf16[16,8,256]{2,1,0:T(8,128)(2,1)S(1)}, u32[]{:S(2)}, u32[]{:S(2)}) async-start(bf16[16,8,256]{2,1,0:T(8,128)(2,1)} %fusion.1), calls=%async_computation | async-start | bytes 131072 | tf_op jit(solution)/shard_map/all_to_all | solution.py:108
  60.1 74.9 %reduce-scatter.3.cloned.1.call-start = ((), (), s32[]{:S(2)}) async-start(), calls=%async_computation.6 | async-start | bytes 49152 | tf_op jit(solution)/shard_map/reduce_scatter | solution.py:140
  67.1 1.3 copy-start.6
  73.4 11.0 %copy-start.2 = (bf16[8,3,2048]{2,0,1:T(8,128)(2,1)S(1)}, bf16[8,3,2048]{2,0,1:T(8,128)(2,1)}, u32[]{:S(2)}) copy-start(bf16[8,3,2048]{2,0,1:T(8,128)(2,1)} %param.42) | copy-start | bytes 294916
  73.4 80.4 %copy-start.5 = (f32[2048]{0:T(1024)S(1)}, f32[2048]{0:T(1024)}, u32[]{:S(2)}) copy-start(f32[2048]{0:T(1024)} %param.49) | copy-start | bytes 24580
  82.8 105.5 %copy-start.1 = (bf16[256,2048]{1,0:T(8,128)(2,1)S(1)}, bf16[256,2048]{1,0:T(8,128)(2,1)}, u32[]{:S(2)}) copy-start(bf16[256,2048]{1,0:T(8,128)(2,1)} %param.57) | copy-start | bytes 3145732
  136.4 14.0 %all-to-all-start.1 = ((bf16[16,4,128]{2,1,0:T(4,128)(2,1)}), bf16[16,4,128]{2,1,0:T(4,128)(2,1)S(1)}, u32[]{:S(2)}, u32[]{:S(2)}) async-start(bf16[16,4,128]{2,1,0:T(4,128)(2,1)} %copy.99), calls=%async_computation.2 | async-start | bytes 32768 | tf_op jit(solution)/shard_map/all_to_all | solution.py:146
  143.1 36.7 %reduce-scatter.5.cloned.1.call-start = ((), (), s32[]{:S(2)}) async-start(), calls=%async_computation.7 | async-start | bytes 393216 | tf_op jit(solution)/shard_map/reduce_scatter | solution.py:190
  153.2 0.6 copy-start.9
  181.5 14.7 %all-to-all-start.3 = ((bf16[16,1,4,1024]{3,2,1,0:T(4,128)(2,1)}), bf16[16,1,4,1024]{3,2,1,0:T(4,128)(2,1)S(1)}, u32[]{:S(2)}, u32[]{:S(2)}) async-start(bf16[16,1,4,1024]{3,2,1,0:T(4,128)(2,1)} %copy.106), calls=%async_computation.5 | async-start | bytes 262144 | tf_op jit(solution)/shard_map/all_to_all | solution.py:193
Sparse Core Ops, SparseCore 0:
  131.6 3.4 reduce-scatter.2
  174.6 5.2 reduce-scatter.4
where the time goes:
time: 208 us; the launch traced here: 206 us
  blocking collectives  109 us (52%)
  other arithmetic  23.6 us (11%)
  starting transfers between devices  17 us (8%)
  matrix products  16.5 us (8%)
  between operations  14.4 us (7%)
  local copies, waits for them, and re-layouts  13.5 us (6%)
  waiting for transfers between devices  12.3 us (6%)
    all_gather x1, blocking collectives, shards(): lax.all_gather(normed, 'ep', axis=0, tiled=True)  45.3 us
    all_gather x1, blocking collectives, shards(): lax.all_gather(mixer_rows, 'ep', axis=0, tiled=True)  44.1 us
    all_to_all x1, blocking collectives, shards(): lax.all_to_all(own_cols, 'ep', split_axis=0, concat_axis=0, tiled=True)  10.6 us
    reduce_sum x1, other arithmetic, state_step(): jnp.sum(state_next * output_heads[:, :, None, :], axis=-1)  9.36 us
    all_to_all x1, starting transfers between devices, shards(): lax.all_to_all(share_out, 'ep', split_axis=0, concat_axis=0, tiled=True)  6.73 us
    all_to_all x1, starting transfers between devices, shards(): lax.all_to_all(mix_share, 'ep', split_axis=0, concat_axis=2, tiled=True)  6.69 us
    all_to_all x1, waiting for transfers between devices, shards(): lax.all_to_all(mix_share, 'ep', split_axis=0, concat_axis=2, tiled=True)  6.62 us
  transfers between devices with their start and end apart: 5, of which 4 were waited for; matrix products, arithmetic and copies ran while one was open for 8% of the time, Pallas kernels for 0%

commit v1 on v0

--- a/solution.py
+++ b/solution.py
@@ -143,7 +143,10 @@
         scatter_dimension=1,
         tiled=True,
     )
-    moved_mix = lax.all_to_all(mix_share, "ep", split_axis=0, concat_axis=2, tiled=True)
+    moved_mix = jnp.concatenate(
+        lax.all_to_all(jnp.stack(jnp.split(mix_share, lax.axis_size("ep"), axis=0)), "ep", 0, 0),
+        axis=2,
+    )
     mixed_out = lax.all_gather(moved_mix, "tp", axis=1, tiled=True).reshape(seq_rows, model_width)
     stream = (tokens.astype(jnp.float32) + mixed_out.astype(jnp.float32)).astype(jnp.bfloat16)
     ffn_rows = rms_scale(stream, expert_norm_gain).astype(jnp.bfloat16)

time: 208 us -> 217 us (1.043)
  local copies, waits for them, and re-layouts: 13.5 us -> 22.2 us
    unnamed x30 -> x45, local copies, waits for them, and re-layouts: 1.51 us -> 9.96 us
where the time goes in v1:
time: 217 us; the launch traced here: 215 us
  blocking collectives  109 us (50%)
  other arithmetic  23.6 us (11%)
  local copies, waits for them, and re-layouts  22.2 us (10%)
  starting transfers between devices  17 us (8%)
  matrix products  16.5 us (8%)
  between operations  14.4 us (7%)
  waiting for transfers between devices  12.3 us (6%)
    all_gather x1, blocking collectives, shards(): lax.all_gather(normed, 'ep', axis=0, tiled=True)  45.3 us
    all_gather x1, blocking collectives, shards(): lax.all_gather(mixer_rows, 'ep', axis=0, tiled=True)  44.1 us
    all_to_all x1, blocking collectives, shards(): lax.all_to_all(own_cols, 'ep', split_axis=0, concat_axis=0, tiled=True)  10.6 us
    unnamed x45, local copies, waits for them, and re-layouts  9.96 us
    reduce_sum x1, other arithmetic, state_step(): jnp.sum(state_next * output_heads[:, :, None, :], axis=-1)  9.36 us
    all_to_all x1, starting transfers between devices, shards(): lax.all_to_all(share_out, 'ep', split_axis=0, concat_axis=0, tiled=True)  6.75 us
    all_to_all x1, starting transfers between devices, shards(): lax.all_to_all(jnp.stack(jnp.split(mix_share, lax.axis_size('ep'), axis=0...  6.69 us
    all_to_all x1, waiting for transfers between devices, shards(): lax.all_to_all(jnp.stack(jnp.split(mix_share, lax.axis_size('ep'), axis=0...  6.62 us
  transfers between devices with their start and end apart: 5, of which 4 were waited for; matrix products, arithmetic and copies ran while one was open for 8% of the time, Pallas kernels for 0%

profile of v1, /device:TPU:0, one launch (start us, length us, event | category | flops | bytes accessed | tf_op | source)
XLA Modules:
  0.0 215.1 jit_solution(39383013531218565)
XLA Ops:
  7.3 1.0 fusion.18
  8.3 0.8 fusion.20
  9.1 45.3 %all_gather.15 = bf16[128,2048]{1,0:T(8,128)(2,1)S(1)} all-gather(bf16[8,2048]{1,0:T(8,128)(2,1)S(1)} %fusion.20), channel_id=1, replica_groups=mesh['ep'=16,'tp'=2] {'ep'}, dimensions={0}, use_global_device_ids=true | all-gather | bytes 557056 | tf_op jit(solution)/shard_map/all_gather | solution.py:104
  54.5 2.2 %fusion.1 = bf16[16,8,256]{2,1,0:T(8,128)(2,1)} fusion(bf16[128,2048]{1,0:T(8,128)(2,1)S(1)} %all_gather.15, bf16[2048,128]{1,0:T(8,128)(2,1)} %bitcast.273, bf16[2048,128]{1,0:T(8,128)(2,1)} %bitcast.274), kind=kOutput, calls=%fused_computation.7 | convolution fusion | flops 136347648 | bytes 1638400 | tf_op jit(solution)/shard_map/dot_general | solution.py:103
  56.6 3.5 %all-to-all-start = ((bf16[16,8,256]{2,1,0:T(8,128)(2,1)}), bf16[16,8,256]{2,1,0:T(8,128)(2,1)S(1)}, u32[]{:S(2)}, u32[]{:S(2)}) async-start(bf16[16,8,256]{2,1,0:T(8,128)(2,1)} %fusion.1), calls=%async_computation | async-start | bytes 131072 | tf_op jit(solution)/shard_map/all_to_all | solution.py:108
  60.2 1.6 slice_reduce_fusion.3
  62.0 0.8 slice_convert_fusion.2
  63.5 0.9 fusion.69
  64.3 0.8 multiply_bitcast_fusion.1
  65.1 2.0 convolution_convert_fusion.6
  67.2 0.7 mul.467
  68.3 0.7 reduce_sum.82
  69.3 0.9 slice_reduce_fusion.4
  70.1 1.0 fusion.65
  71.1 0.8 copy_convert_fusion
  72.0 0.7 reshape.336
  72.7 0.7 broadcast_multiply_fusion
  73.4 9.4 %multiply_reduce_fusion = (f32[8,32,64]{2,1,0:T(8,128)S(1)}, f32[8,32,64,128]{3,2,1,0:T(8,128)}) fusion(f32[8,32,128]{2,1,0:T(8,128)S(1)} %get-tuple-element.57, f32[8,32,128]{2,1,0:T(8,128)S(1)} %get-tuple-element.58, f32[8,32,64]{2,1,0:T(8,128)S(1)} %get-tuple-element.15, f32[8,32,64,128]{3,2,1,0:T(8,128)} %param.48, f32[8,32]{1,0:T(8,128)S(1)} %get-tuple-element.51), kind=kLoop, calls=%fused_computation | loop fusion | flops 10469376 | bytes 17171456 | tf_op jit(solution)/shard_map/reduce_sum | solution.py:39
  82.9 1.2 multiply_reduce_fusion.1
  84.4 1.0 fusion.41
  85.4 44.1 %all_gather.16 = bf16[128,2048]{1,0:T(8,128)(2,1)S(1)} all-gather(bf16[8,2048]{1,0:T(8,128)(2,1)S(1)} %fusion.41), channel_id=1, replica_groups=mesh['ep'=16,'tp'=2] {'ep'}, dimensions={0}, use_global_device_ids=true | all-gather | bytes 557056 | tf_op jit(solution)/shard_map/all_gather | solution.py:136
  129.5 1.3 fusion.5
  130.8 0.6 copy.131
  131.5 0.7 multiply_add_fusion.1
  132.3 0.8 copy.150
  133.0 2.0 reduce-scatter.3.cloned.1.call-done
  135.1 1.1 fusion.68
  136.2 0.6 constant_dynamic-update-slice_fusion.15
  136.7 0.6 constant_dynamic-update-slice_fusion.14
  137.3 0.6 constant_dynamic-update-slice_fusion.13
  137.8 0.6 constant_dynamic-update-slice_fusion.12
  138.4 0.6 constant_dynamic-update-slice_fusion.11
  139.0 0.6 constant_dynamic-update-slice_fusion.10
  139.5 0.6 constant_dynamic-update-slice_fusion.9
  140.1 0.6 constant_dynamic-update-slice_fusion.8
  140.7 0.6 constant_dynamic-update-slice_fusion.7
  141.2 0.6 constant_dynamic-update-slice_fusion.6
  142.9 0.6 constant_dynamic-update-slice_fusion.3
  144.1 0.6 constant_dynamic-update-slice_fusion.1
  145.2 6.7 %all-to-all-start.1 = ((bf16[16,1,4,128]{3,2,1,0:T(4,128)(2,1)}), bf16[16,1,4,128]{3,2,1,0:T(4,128)(2,1)S(1)}, u32[]{:S(2)}, u32[]{:S(2)}) async-start(bf16[16,1,4,128]{3,2,1,0:T(4,128)(2,1)} %constant_dynamic-update-slice_fusion), calls=%async_computation.2 | async-start | bytes 32768 | tf_op jit(solution)/shard_map/all_to_all | solution.py:147
  151.9 0.7 convert_reduce_fusion
  152.6 6.6 %all-to-all-done.1 = bf16[16,1,4,128]{3,2,1,0:T(4,128)(2,1)S(1)} async-done(((bf16[16,1,4,128]{3,2,1,0:T(4,128)(2,1)}), bf16[16,1,4,128]{3,2,1,0:T(4,128)(2,1)S(1)}, u32[]{:S(2)}, u32[]{:S(2)}) %all-to-all-start.1) | async-done | bytes 16416 | tf_op jit(solution)/shard_map/all_to_all | solution.py:147
  159.2 1.9 all_gather.17
  161.1 0.9 fusion.22
  162.0 0.6 copy-done.9
  162.6 1.0 convolution_convert_fusion.1
  163.6 0.8 reshape.314
  164.4 0.9 constant_dynamic-slice_fusion
  165.3 10.6 %all_to_all.31 = bf16[16,1,4,1024]{3,2,1,0:T(4,128)(2,1)S(1)} all-to-all(bf16[16,1,4,1024]{3,2,1,0:T(4,128)(2,1)S(1)} %constant_dynamic-slice_fusion), channel_id=1, replica_groups=mesh['ep'=16,'tp'=2] {'ep'}, dimensions={0} | all-to-all | bytes 262144 | tf_op jit(solution)/shard_map/all_to_all | solution.py:185
  176.0 2.0 all_gather.18
  178.0 2.1 convolution_bitcast_fusion.1
  180.1 3.1 %fusion = bf16[16,1,4,2048]{3,0,2,1:T(8,128)(2,1)} fusion(bf16[1,256,2048]{2,1,0:T(8,128)(2,1)} %param.54, bf16[1,2048,256]{2,1,0:T(8,128)(2,1)} %param.53, bf16[16,1,4,2048]{3,0,2,1:T(8,128)(2,1)S(1)} %all_gather.18, f32[16,1,4,256]{3,0,2,1:T(8,128)} %convolution_bitcast_fusion.1), kind=kOutput, calls=%fused_computation.4 | convolution fusion | flops 134447104 | bytes 2686976 | tf_op jit(solution)/shard_map/slcf,lfd->slcd/dot_general | solution.py:56
  183.2 1.4 pad_maximum_fusion.1
  184.6 1.4 pad_maximum_fusion
  186.0 1.5 fusion.63
  187.6 1.0 reduce-scatter.5.cloned.1.call-done
  188.6 1.6 copy.153
  190.3 6.7 %all-to-all-start.3 = ((bf16[16,1,4,1024]{3,2,1,0:T(4,128)(2,1)}), bf16[16,1,4,1024]{3,2,1,0:T(4,128)(2,1)S(1)}, u32[]{:S(2)}, u32[]{:S(2)}) async-start(bf16[16,1,4,1024]{3,2,1,0:T(4,128)(2,1)} %copy.153), calls=%async_computation.5 | async-start | bytes 262144 | tf_op jit(solution)/shard_map/all_to_all | solution.py:196
  197.0 2.0 convolution_convert_fusion.2
  199.0 3.4 %psum.7 = bf16[8,2048]{1,0:T(8,128)(2,1)S(1)} all-reduce(bf16[8,2048]{1,0:T(8,128)(2,1)S(1)} %convolution_convert_fusion.2), channel_id=1, replica_groups=mesh['ep'=16,'tp'=2] {'tp'}, use_global_device_ids=true, to_apply=%region_6.7 | all-reduce | flops 16384 | bytes 65536 | tf_op jit(solution)/shard_map/psum | solution.py:157
  202.4 2.5 %all-to-all-done.3 = bf16[16,1,4,1024]{3,2,1,0:T(4,128)(2,1)S(1)} async-done(((bf16[16,1,4,1024]{3,2,1,0:T(4,128)(2,1)}), bf16[16,1,4,1024]{3,2,1,0:T(4,128)(2,1)S(1)}, u32[]{:S(2)}, u32[]{:S(2)}) %all-to-all-start.3) | async-done | bytes 131104 | tf_op jit(solution)/shard_map/all_to_all | solution.py:196
  205.0 0.8 convolution_convert_fusion.5
  205.8 1.8 all_gather.19
  207.6 0.6 fusion.26
  (69 shorter events, 4.8 us)
Async XLA Ops:
  7.2 55.9 %copy-start = (bf16[2048,512]{1,0:T(8,128)(2,1)S(1)}, bf16[2048,512]{1,0:T(8,128)(2,1)}, u32[]{:S(2)}) copy-start(bf16[2048,512]{1,0:T(8,128)(2,1)} %param.33) | copy-start | bytes 6291460
  7.2 59.9 %copy-start.8 = (f32[4,512]{1,0:T(4,128)S(1)}, f32[4,512]{1,0:T(4,128)}, u32[]{:S(2)}) copy-start(f32[4,512]{1,0:T(4,128)} %param.41) | copy-start | bytes 24580
  7.2 59.9 %copy-start.4 = (bf16[8,3,512]{2,0,1:T(8,128)(2,1)S(1)}, bf16[8,3,512]{2,0,1:T(8,128)(2,1)}, u32[]{:S(2)}) copy-start(bf16[8,3,512]{2,0,1:T(8,128)(2,1)} %param.44) | copy-start | bytes 73732
  7.2 60.0 %copy-start.11 = (f32[32]{0:T(128)S(1)}, f32[32]{0:T(128)}, u32[]{:S(2)}) copy-start(f32[32]{0:T(128)} %param.45) | copy-start | bytes 388
  7.2 60.7 %copy-start.7 = (s32[8,6]{1,0:T(8,128)S(1)}, s32[8,6]{1,0:T(8,128)}, u32[]{:S(2)}) copy-start(s32[8,6]{1,0:T(8,128)} %param.50) | copy-start | bytes 580
  7.2 61.8 %copy-start.3 = (bf16[2048,32]{0,1:T(8,128)(2,1)S(1)}, bf16[2048,32]{0,1:T(8,128)(2,1)}, u32[]{:S(2)}) copy-start(bf16[2048,32]{0,1:T(8,128)(2,1)} %param.35) | copy-start | bytes 393220
  7.2 61.8 %copy-start.13 = (f32[32]{0:T(128)S(1)}, f32[32]{0:T(128)}, u32[]{:S(2)}) copy-start(f32[32]{0:T(128)} %param.36) | copy-start | bytes 388
  7.2 61.8 %copy-start.12 = (f32[32]{0:T(128)S(1)}, f32[32]{0:T(128)}, u32[]{:S(2)}) copy-start(f32[32]{0:T(128)} %param.37) | copy-start | bytes 388
  7.3 61.8 %copy-start.10 = (f32[8,32]{1,0:T(8,128)S(1)}, f32[8,32]{1,0:T(8,128)}, u32[]{:S(2)}) copy-start(f32[8,32]{1,0:T(8,128)} %param.38) | copy-start | bytes 3076
  56.6 12.6 %all-to-all-start = ((bf16[16,8,256]{2,1,0:T(8,128)(2,1)}), bf16[16,8,256]{2,1,0:T(8,128)(2,1)S(1)}, u32[]{:S(2)}, u32[]{:S(2)}) async-start(bf16[16,8,256]{2,1,0:T(8,128)(2,1)} %fusion.1), calls=%async_computation | async-start | bytes 131072 | tf_op jit(solution)/shard_map/all_to_all | solution.py:108
  60.1 74.9 %reduce-scatter.3.cloned.1.call-start = ((), (), s32[]{:S(2)}) async-start(), calls=%async_computation.6 | async-start | bytes 49152 | tf_op jit(solution)/shard_map/reduce_scatter | solution.py:140
  67.1 1.3 copy-start.6
  73.4 11.0 %copy-start.2 = (bf16[8,3,2048]{2,0,1:T(8,128)(2,1)S(1)}, bf16[8,3,2048]{2,0,1:T(8,128)(2,1)}, u32[]{:S(2)}) copy-start(bf16[8,3,2048]{2,0,1:T(8,128)(2,1)} %param.42) | copy-start | bytes 294916
  73.4 89.2 %copy-start.5 = (f32[2048]{0:T(1024)S(1)}, f32[2048]{0:T(1024)}, u32[]{:S(2)}) copy-start(f32[2048]{0:T(1024)} %param.49) | copy-start | bytes 24580
  82.8 114.2 %copy-start.1 = (bf16[256,2048]{1,0:T(8,128)(2,1)S(1)}, bf16[256,2048]{1,0:T(8,128)(2,1)}, u32[]{:S(2)}) copy-start(bf16[256,2048]{1,0:T(8,128)(2,1)} %param.57) | copy-start | bytes 3145732
  145.2 14.0 %all-to-all-start.1 = ((bf16[16,1,4,128]{3,2,1,0:T(4,128)(2,1)}), bf16[16,1,4,128]{3,2,1,0:T(4,128)(2,1)S(1)}, u32[]{:S(2)}, u32[]{:S(2)}) async-start(bf16[16,1,4,128]{3,2,1,0:T(4,128)(2,1)} %constant_dynamic-update-slice_fusion), calls=%async_computation.2 | async-start | bytes 32768 | tf_op jit(solution)/shard_map/all_to_all | solution.py:147
  151.9 36.7 %reduce-scatter.5.cloned.1.call-start = ((), (), s32[]{:S(2)}) async-start(), calls=%async_computation.7 | async-start | bytes 393216 | tf_op jit(solution)/shard_map/reduce_scatter | solution.py:193
  162.0 0.6 copy-start.9
  190.3 14.7 %all-to-all-start.3 = ((bf16[16,1,4,1024]{3,2,1,0:T(4,128)(2,1)}), bf16[16,1,4,1024]{3,2,1,0:T(4,128)(2,1)S(1)}, u32[]{:S(2)}, u32[]{:S(2)}) async-start(bf16[16,1,4,1024]{3,2,1,0:T(4,128)(2,1)} %copy.153), calls=%async_computation.5 | async-start | bytes 262144 | tf_op jit(solution)/shard_map/all_to_all | solution.py:196
Sparse Core Ops, SparseCore 0:
  131.6 3.4 reduce-scatter.2
  183.4 5.2 reduce-scatter.4
